TPU v7x, 512 devices: a 4x2x32 block of a 4x8x32 slice. The times are simulated.
512 devices in a mesh: grp: 2 (over y), sp: 32 (over z), tp: 8 (over x, core).
Axes of the slice: x: 4, y: 2, z: 32, core: 2. Of those that a mesh axis runs over, the one named last changes fastest.
The devices are a block of a 4x8x32 slice.
Arguments:
- prompt: bfloat16 [8, 6144, 2048], P('grp', 'sp'), parts along dimension 0, may hold values from -6 to 6
- w_key: bfloat16 [2048, 2048], P('sp', 'tp'), may hold values from -0.125 to 0.125
- w_value: bfloat16 [2048, 2048], P('sp', 'tp'), may hold values from -0.125 to 0.125
- query_new: bfloat16 [8, 2048], P('grp', 'tp'), parts along dimension 0, may hold values from -150 to 150
- key_new: bfloat16 [8, 2048], P('grp', 'tp'), parts along dimension 0, may hold values from -15 to 15
- value_new: bfloat16 [8, 2048], P('grp', 'tp'), parts along dimension 0, may hold values from -6 to 6
- mix_lambda: float32 [16], P('tp'), may hold values from 0.3 to 0.8
- head_gain: float32 [128], replicated, may hold values from 0.1 to 1.9
Outputs:
- key_cache: bfloat16 [64, 32, 24, 2048], P(('grp', 'sp'), None, None, 'tp'), parts along dimension 0
- value_cache: bfloat16 [64, 32, 24, 2048], P(('grp', 'sp'), None, None, 'tp'), parts along dimension 0
- first_read: bfloat16 [8, 2048], P('grp', 'tp'), parts along dimension 0
There are 2 independent parts, one for each index of `grp`. A program takes and returns all parts, laid end to end along the dimension named above; an argument that names none is the same for every part. Nothing has to cross between parts.
All inputs are finite; a program needn't handle non-finite values.
Results may differ from a plain program's by a relative error of at most 0.0065.
The roundings to bfloat16 on the way count: a program that leaves them out, or rounds other values in their place, can miss the bound.
Values may be sent and summed in bfloat16 or wider, within the bound.
No kernel may reach another device: no remote copies, remote signals or barrier semaphores. Data moves between devices by JAX's collectives and lax.ppermute only.
A program may use at most 64 MiB of HBM per device.

v0:
```python
import functools
import jax
import jax.numpy as jnp
from jax import lax
from jax.experimental import pallas as pl
from jax.experimental.pallas import tpu as pltpu
from jax.sharding import PartitionSpec as P

HALF = 64
VDIM = 128
W_SHIFT = 2.0**18
F32 = jnp.float32
BF16 = jnp.bfloat16
NEG = -1e30


def row_dot(a, b, precision=None):
    return lax.dot_general(a, b, (((1,), (1,)), ((), ())), preferred_element_type=F32, precision=precision)


def select_rows(rows, query, count, heads, pairs):
    width = query.shape[1]
    r = lax.broadcasted_iota(jnp.int32, (rows, width), 0)
    lane = lax.broadcasted_iota(jnp.int32, (rows, width), 1)
    out = jnp.zeros((rows, width), F32)
    for b in range(count):
        q = jnp.broadcast_to(query[b : b + 1, :].astype(F32), (rows, width))
        out = jnp.where((r // heads) % count == b, q, out)
    slot = (r % heads) * pairs + r // (count * heads)
    return jnp.where(lane // HALF == slot, out, 0.0)


def local_kernel(heads, x_ref, w_ref, q_ref, pay_ref):
    count, piece, width = x_ref.shape
    rows = 2 * count * heads
    cols = heads * 2 * HALF
    x = x_ref[...].reshape(count * piece, width)
    keys = jnp.dot(x, w_ref[:, :cols], preferred_element_type=F32).astype(BF16)
    values = jnp.dot(x, w_ref[:, cols:], preferred_element_type=F32).astype(BF16)
    picked = select_rows(rows, q_ref[...], count, heads, 2)
    scores = row_dot(picked.astype(BF16), keys) * HALF**-0.5
    r = lax.broadcasted_iota(jnp.int32, scores.shape, 0)
    at = lax.broadcasted_iota(jnp.int32, scores.shape, 1)
    scores = jnp.where((r // heads) % count == at // piece, scores, NEG)
    top = jnp.max(scores, axis=1, keepdims=True)
    weights = jnp.exp(scores - top)
    total = jnp.sum(weights, axis=1, keepdims=True)
    full = 0.0
    for p in three(weights):
        full += jnp.dot(p, values, preferred_element_type=F32)
    r = lax.broadcasted_iota(jnp.int32, (rows, VDIM), 0)
    part = jnp.zeros((rows, VDIM), F32)
    for h in range(heads):
        part = jnp.where(r % heads == h, full[:, h * VDIM : (h + 1) * VDIM], part)
    part = part / total
    power = jnp.ceil(jnp.log2(jnp.maximum(jnp.max(jnp.abs(part), axis=1, keepdims=True), 1e-30)))
    pay_ref[:rows, :] = part * jnp.exp2(-power)
    pay_ref[rows:, :] = jnp.zeros((pay_ref.shape[0] - rows, VDIM), F32)
    pieces = [p.astype(F32) * 256.0**n for x in (top / 64, total) for n, p in enumerate(three(x))]
    pay_ref[rows : rows + 1, :] = as_line([*pieces, power])


def three(x):
    high = x.astype(BF16)
    rest = x - high.astype(F32)
    middle = rest.astype(BF16)
    return high, middle, (rest - middle.astype(F32)).astype(BF16)


def as_line(columns):
    rows = sum(c.shape[0] for c in columns)
    both = jnp.concatenate([*columns, jnp.zeros((VDIM - rows, 1), F32)], axis=0)
    return jnp.broadcast_to(both, (VDIM, VDIM)).T[:1]


def fresh_kernel(heads, lam_ref, q_ref, kn_ref, vn_ref, gain_ref, out_ref):
    count = vn_ref.shape[0]
    half = count * heads
    rows = 2 * half
    fresh = select_rows(rows, q_ref[...], count, heads, 2) * select_rows(rows, kn_ref[...], count, heads, 2)
    out_ref[0:1, :] = as_line([jnp.sum(fresh, axis=1, keepdims=True) * HALF**-0.5])
    lane = lax.broadcasted_iota(jnp.int32, (1, VDIM), 1)
    sign = jnp.ones((1, VDIM), F32)
    for h in range(heads):
        sign = jnp.where((lane >= half) & (lane % heads == h), -lam_ref[h], sign)
    out_ref[1:2, :] = sign
    out_ref[2:3, :] = gain_ref[...]
    out_ref[3:8, :] = jnp.zeros((5, VDIM), F32)
    values = vn_ref[...].astype(F32)
    for b in range(count):
        for h in range(heads):
            n = 8 + b * heads + h
            out_ref[n : n + 1, :] = values[b : b + 1, h * VDIM : (h + 1) * VDIM]


def row_of_each(part_ref, r):
    each = part_ref.shape[2] // VDIM
    return part_ref[r // each, :, (r % each) * VDIM : (r % each + 1) * VDIM]


def finish_kernel(heads, part_ref, new_ref, out_ref):
    count = out_ref.shape[0]
    half = count * heads
    rows = 2 * half
    fresh = new_ref[0:1, :]
    stats = row_of_each(part_ref, rows)
    piece = [pltpu.roll(stats, (VDIM - n * rows) % VDIM, 1) for n in range(7)]
    tops = (piece[0] + piece[1] / 256.0 + piece[2] / 65536.0) * 64
    totals = piece[3] + piece[4] / 256.0 + piece[5] / 65536.0
    power = piece[6]
    top = jnp.maximum(jnp.max(tops, axis=0, keepdims=True), fresh)
    scale = jnp.exp(jnp.minimum(tops - top, 0.0))
    own = jnp.exp(fresh - top)
    total = jnp.sum(totals * scale, axis=0, keepdims=True) + own
    scale = scale * totals * jnp.exp2(power) * (new_ref[1:2, :] / total)
    own = own * (new_ref[1:2, :] / total)
    mine = (own + pltpu.roll(own, VDIM - half, 1)).astype(BF16).astype(F32)
    for b in range(count):
        for h in range(heads):
            n = b * heads + h
            reads = 0.0
            for r in (n, n + half):
                reads += scale[:, r : r + 1] * row_of_each(part_ref, r)
            reads = jnp.sum(reads, axis=0, keepdims=True)
            reads += mine[:, n : n + 1] * new_ref[8 + n : 9 + n, :]
            mean = jnp.mean(reads * reads, axis=1, keepdims=True)
            normed = reads * lax.rsqrt(mean + 1e-06) * new_ref[2:3, :]
            out_ref[b : b + 1, h * VDIM : (h + 1) * VDIM] = normed.astype(BF16)


def slices_kernel(chips, x_refs, w_ref, where, acc_ref, x_buf, w_buf, sem):
    rows = x_refs[0].shape[0]
    moves = []
    for n in range(chips):
        moves.append(
            [
                pltpu.make_async_copy(w_ref.at[where(n)], w_buf.at[n], sem.at[n, 0]),
                pltpu.make_async_copy(x_refs[n], x_buf.at[n], sem.at[n, 1]),
            ]
        )
        for m in moves[n]:
            m.start()
    step = rows // 4
    for at in range(0, rows, step):
        acc = 0.0
        for n in range(chips):
            if at == 0:
                for m in moves[n]:
                    m.wait()
            acc += jnp.dot(x_buf[n, at : at + step, :], w_buf[n], preferred_element_type=F32)
        acc_ref[at : at + step, :] = acc


def theirs_kernel(chips, *refs):
    t = lax.axis_index("tp")
    where = lambda n: lax.div(lax.rem(t + 2 * chips - 2 * n, 2 * chips), 2)
    slices_kernel(chips, refs[:chips], refs[chips], where, *refs[chips + 1 :])


def ours_kernel(chips, *refs):
    t = lax.axis_index("tp")
    where = lambda n: lax.rem(t + 2 * chips - 2 * n, 2 * chips)
    slices_kernel(chips, refs[:chips], refs[chips], where, *refs[chips + 1 :])


def join_kernel(ours_ref, swapped_ref, k_ref, v_ref):
    cols = k_ref.shape[1]
    k_ref[...] = (ours_ref[:, :cols] + swapped_ref[:, :cols]).astype(BF16)
    v_ref[...] = (ours_ref[:, cols:] + swapped_ref[:, cols:]).astype(BF16)


def call(kernel, outs, args, spaces="", scratch=(), limit=16):
    kinds = {"s": pltpu.SMEM, "a": pl.ANY, "v": pltpu.VMEM}
    spaces = spaces.ljust(len(args), "v")
    return pl.pallas_call(
        kernel,
        out_shape=[jax.ShapeDtypeStruct(s, d) for s, d in outs],
        in_specs=[pl.BlockSpec(memory_space=kinds[c]) for c in spaces],
        out_specs=[pl.BlockSpec(memory_space=pltpu.VMEM)] * len(outs),
        scratch_shapes=scratch,
        compiler_params=pltpu.CompilerParams(vmem_limit_bytes=int(limit * 2**20)),
    )(*args)


def spread(x, axis):
    return lax.all_to_all(x, axis, 0, 0, tiled=True)


def moved(x, axis, step):
    n = lax.axis_size(axis)
    return lax.ppermute(x, axis, [(i, step(i) % n) for i in range(n)])


def inner(prompt, w_key, w_value, query_new, key_new, value_new, mix_lambda, head_gain):
    count, piece, width = prompt.shape
    peers = lax.axis_size("sp")
    slices = lax.axis_size("tp")
    groups = peers // count
    sub = piece // groups
    heads = mix_lambda.shape[0]
    cols = w_key.shape[1]
    half = count * heads
    t = lax.axis_index("tp")

    depth = width // slices
    mine = lax.dynamic_slice_in_dim(prompt, t * depth, depth, 2).reshape(peers, sub, depth)
    w = jnp.concatenate([w_key, w_value], axis=1)
    w = (w.astype(F32) * W_SHIFT).astype(jnp.float16)
    mine, w = lax.optimization_barrier((mine, w))
    w = lax.all_gather(w, "sp", axis=0, tiled=True)
    w = (w.astype(F32) * (1 / W_SHIFT)).astype(BF16)

    (fresh,) = call(
        functools.partial(fresh_kernel, heads),
        [((8 + half, VDIM), F32)],
        (mix_lambda, query_new, key_new, value_new, head_gain.reshape(1, VDIM)),
        "s",
    )
    each = half + 1
    (pay,) = call(functools.partial(local_kernel, heads), [((2 * each, VDIM), F32)], (prompt, w, query_new))
    pay, mine = lax.optimization_barrier((pay, mine))
    mine = spread(mine, "sp").reshape(peers * sub, depth)
    parts = jnp.broadcast_to(pay.reshape(2, each * VDIM).astype(jnp.float16), (peers, 2, each * VDIM))
    parts = spread(parts, "sp")
    parts = parts.astype(F32).transpose(1, 0, 2)
    (first_read,) = call(functools.partial(finish_kernel, heads), [((count, cols), BF16)], (parts, fresh))

    chips = slices // 2
    w = w.reshape(slices, depth, 2 * cols)
    lent = lax.dynamic_index_in_dim(w.reshape(chips, 2, depth, 2 * cols), 1 - t % 2, 1, False)
    lent = moved(lent, "tp", lambda i: i ^ 1)
    found = [mine]
    for d in range(1, chips):
        found.append(moved(mine, "tp", lambda i: i + 2 * d))
    scratch = [
        pltpu.VMEM((chips, peers * sub, depth), BF16),
        pltpu.VMEM((chips, depth, 2 * cols), BF16),
        pltpu.SemaphoreType.DMA((chips, 2)),
    ]
    partial = [((peers * sub, 2 * cols), F32)]
    anywhere = "a" * (chips + 1)
    (theirs,) = call(functools.partial(theirs_kernel, chips), partial, (*found, lent), anywhere, scratch)
    theirs = moved(theirs, "tp", lambda i: i ^ 1)
    (ours,) = call(functools.partial(ours_kernel, chips), partial, (*found, w), anywhere, scratch)
    key_cache, value_cache = call(join_kernel, [((peers * sub, cols), BF16)] * 2, (ours, theirs))
    shape = (1, peers, sub, cols)
    return key_cache.reshape(shape), value_cache.reshape(shape), first_read


def solution(mesh):
    return jax.shard_map(
        inner,
        mesh=mesh,
        in_specs=(
            P("grp", "sp", None),
            P("sp", "tp"),
            P("sp", "tp"),
            P("grp", "tp"),
            P("grp", "tp"),
            P("grp", "tp"),
            P("tp"),
            P(),
        ),
        out_specs=(
            P(("grp", "sp"), None, None, "tp"),
            P(("grp", "sp"), None, None, "tp"),
            P("grp", "tp"),
        ),
        check_vma=False,
    )
```

profile of v0, /device:TPU:40, one launch (start us, length us, event | category | flops | bytes accessed | tf_op | source)
XLA Modules:
  0.0 211.1 jit_solution(7477376897280055907)
XLA Ops:
  0.6 1.8 constant_dynamic-slice_fusion
  2.4 0.8 multiply_convert_fusion.1
  3.2 107.4 %all-gather.1 = f16[2048,512]{1,0:T(8,128)(2,1)S(1)} all-gather(f16[64,512]{1,0:T(8,128)(2,1)S(1)} %multiply_convert_fusion.1), channel_id=1, replica_groups=mesh['grp'=2,'sp'=32,'tp'=8] {'sp'}, dimensions={0}, use_global_device_ids=true | all-gather | bytes 2162688 | tf_op jit(solution)/shard_map/all_gather | solution.py:210
  110.6 0.5 multiply_convert_fusion.w_ref
  111.1 1.4 copy-done
  112.5 0.0 copy-done.1
  112.5 2.7 %shard_map.103 = f32[18,128]{1,0:T(8,128)S(1)} custom-call(bf16[4,192,2048]{2,1,0:T(8,128)(2,1)S(1)} %copy-done, bf16[2048,512]{1,0:T(8,128)(2,1)S(1)} %multiply_convert_fusion.w_ref, bf16[4,256]{1,0:T(4,128)(2,1)S(1)} %copy-done.1), custom_call_target="tpu_custom_call" | custom-call | tf_op jit(solution)/shard_map/pallas_call | solution.py:175
  115.2 6.0 %all-to-all-start = ((bf16[32,24,256]{2,1,0:T(8,128)(2,1)}), bf16[32,24,256]{2,1,0:T(8,128)(2,1)S(1)}, u32[]{:S(2)}, u32[]{:S(2)}) async-start(bf16[32,24,256]{2,1,0:T(8,128)(2,1)} %bitcast), calls=%async_computation | async-start | bytes 786432 | tf_op jit(solution)/shard_map/all_to_all | solution.py:186
  121.2 1.1 dynamic-slice_bitcast_fusion
  122.2 1.9 collective-permute-start.3
  124.2 36.4 %all-to-all-done = bf16[32,24,256]{2,1,0:T(8,128)(2,1)S(1)} async-done(((bf16[32,24,256]{2,1,0:T(8,128)(2,1)}), bf16[32,24,256]{2,1,0:T(8,128)(2,1)S(1)}, u32[]{:S(2)}, u32[]{:S(2)}) %all-to-all-start) | async-done | bytes 393248 | tf_op jit(solution)/shard_map/all_to_all | solution.py:186
  160.6 3.5 %collective-permute-start = (bf16[768,256]{1,0:T(8,128)(2,1)S(1)}, bf16[768,256]{1,0:T(8,128)(2,1)S(1)}, u32[]{:S(2)}, u32[]{:S(2)}) collective-permute-start(bf16[768,256]{1,0:T(8,128)(2,1)S(1)} %bitcast.15), channel_id=1, source_target_pairs={{0,2},{1,3},{2,4},{3,5},{4,6},{5,7},{6,0},{7,1},{8,10},{9,11},{10,... | collective-permute-start | bytes 1179656 | tf_op jit(solution)/shard_map/ppermute | solution.py:191
  164.1 4.9 %collective-permute-start.1 = (bf16[768,256]{1,0:T(8,128)(2,1)S(1)}, bf16[768,256]{1,0:T(8,128)(2,1)S(1)}, u32[]{:S(2)}, u32[]{:S(2)}) collective-permute-start(bf16[768,256]{1,0:T(8,128)(2,1)S(1)} %bitcast.16), channel_id=1, source_target_pairs={{0,4},{1,5},{2,6},{3,7},{4,0},{5,1},{6,2},{7,3},{8,12},{9,13},{10,... | collective-permute-start | bytes 1179656 | tf_op jit(solution)/shard_map/ppermute | solution.py:191
  169.1 3.2 %collective-permute-start.2 = (bf16[768,256]{1,0:T(8,128)(2,1)S(1)}, bf16[768,256]{1,0:T(8,128)(2,1)}, u32[]{:S(2)}, u32[]{:S(2)}) collective-permute-start(bf16[768,256]{1,0:T(8,128)(2,1)S(1)} %bitcast.17), channel_id=1, source_target_pairs={{0,6},{1,7},{2,0},{3,1},{4,2},{5,3},{6,4},{7,5},{8,14},{9,15},{10,... | collective-permute-start | bytes 1179656 | tf_op jit(solution)/shard_map/ppermute | solution.py:191
  172.3 0.7 broadcast_in_dim.3
  173.1 4.8 %all-to-all-start.1 = ((f16[32,2,1152]{2,1,0:T(2,128)(2,1)}), f16[32,2,1152]{2,1,0:T(2,128)(2,1)S(1)}, u32[]{:S(2)}, u32[]{:S(2)}) async-start(f16[32,2,1152]{2,1,0:T(2,128)(2,1)} %broadcast_in_dim.3), calls=%async_computation.1 | async-start | bytes 294912 | tf_op jit(solution)/shard_map/all_to_all | solution.py:186
  177.9 0.0 copy-start.2
  177.9 0.0 copy-start.3
  177.9 0.0 copy-start.4
  177.9 0.0 copy-start.5
  177.9 0.0 collective-permute-done.3.refs_4_
  177.9 0.0 collective-permute-done.refs_1_
  177.9 0.0 collective-permute-done.1.refs_2_
  177.9 0.9 collective-permute-done.2.refs_3_
  178.9 3.8 %shard_map.105 = f32[768,512]{1,0:T(8,128)} custom-call(bf16[768,256]{1,0:T(8,128)(2,1)S(1)} %bitcast.18, bf16[768,256]{1,0:T(8,128)(2,1)S(1)} %collective-permute-done.refs_1_, bf16[768,256]{1,0:T(8,128)(2,1)S(1)} %collective-permute-done.1.refs_2_, bf16[768,256]{1,0:T(8,128)(2,1)} %collective-permute-done.2.refs_3_, ...), custom_call_target="tpu_custom_call" | custom-call | tf_op jit(solution)/shard_map/pallas_call | solution.py:175
  182.6 2.0 collective-permute-start.4
  184.6 0.8 shard_map.107.new_ref
  185.4 19.7 %all-to-all-done.1 = f16[32,2,1152]{2,1,0:T(2,128)(2,1)S(1)} async-done(((f16[32,2,1152]{2,1,0:T(2,128)(2,1)}), f16[32,2,1152]{2,1,0:T(2,128)(2,1)S(1)}, u32[]{:S(2)}, u32[]{:S(2)}) %all-to-all-start.1) | async-done | bytes 147488 | tf_op jit(solution)/shard_map/all_to_all | solution.py:186
  205.1 1.0 shard_map.108
  206.1 2.5 %shard_map.104.ours_ref = f32[768,512]{1,0:T(8,128)S(1)} custom-call(bf16[768,256]{1,0:T(8,128)(2,1)S(1)} %bitcast.19, bf16[768,256]{1,0:T(8,128)(2,1)S(1)} %collective-permute-done.refs_1_, bf16[768,256]{1,0:T(8,128)(2,1)S(1)} %collective-permute-done.1.refs_2_, bf16[768,256]{1,0:T(8,128)(2,1)} %collective-permute-done.2.refs_3_, ...), custom_call_target="tpu_custom_call" | custom-call | tf_op jit(solution)/shard_map/pallas_call | solution.py:175
  208.6 0.0 collective-permute-done.4.swapped_ref
  208.7 2.5 %shard_map.106 = (bf16[768,256]{1,0:T(8,128)(2,1)}, bf16[768,256]{1,0:T(8,128)(2,1)}) custom-call(f32[768,512]{1,0:T(8,128)S(1)} %shard_map.104.ours_ref, f32[768,512]{1,0:T(8,128)} %collective-permute-done.4.swapped_ref), custom_call_target="tpu_custom_call" | custom-call | tf_op jit(solution)/shard_map/pallas_call | solution.py:175
  (9 shorter events, 0.1 us)
Async XLA Ops:
  110.6 1.9 copy-start
  110.6 1.9 copy-start.1
  115.2 45.4 %all-to-all-start = ((bf16[32,24,256]{2,1,0:T(8,128)(2,1)}), bf16[32,24,256]{2,1,0:T(8,128)(2,1)S(1)}, u32[]{:S(2)}, u32[]{:S(2)}) async-start(bf16[32,24,256]{2,1,0:T(8,128)(2,1)} %bitcast), calls=%async_computation | async-start | bytes 786432 | tf_op jit(solution)/shard_map/all_to_all | solution.py:186
  122.2 55.7 %collective-permute-start.3 = (bf16[4,256,512]{2,1,0:T(8,128)(2,1)}, bf16[4,256,512]{2,1,0:T(8,128)(2,1)}, u32[]{:S(2)}, u32[]{:S(2)}) collective-permute-start(bf16[4,256,512]{2,1,0:T(8,128)(2,1)} %dynamic-slice_bitcast_fusion), channel_id=1, source_target_pairs={{0,1},{1,0},{2,3},{3,2},{4,5},{5,4},{6,7},{7,6},{8,9},{9,8},{10,11... | collective-permute-start | bytes 3145736 | tf_op jit(solution)/shard_map/ppermute | solution.py:191
  160.6 17.4 %collective-permute-start = (bf16[768,256]{1,0:T(8,128)(2,1)S(1)}, bf16[768,256]{1,0:T(8,128)(2,1)S(1)}, u32[]{:S(2)}, u32[]{:S(2)}) collective-permute-start(bf16[768,256]{1,0:T(8,128)(2,1)S(1)} %bitcast.15), channel_id=1, source_target_pairs={{0,2},{1,3},{2,4},{3,5},{4,6},{5,7},{6,0},{7,1},{8,10},{9,11},{10,... | collective-permute-start | bytes 1179656 | tf_op jit(solution)/shard_map/ppermute | solution.py:191
  164.1 13.8 %collective-permute-start.1 = (bf16[768,256]{1,0:T(8,128)(2,1)S(1)}, bf16[768,256]{1,0:T(8,128)(2,1)S(1)}, u32[]{:S(2)}, u32[]{:S(2)}) collective-permute-start(bf16[768,256]{1,0:T(8,128)(2,1)S(1)} %bitcast.16), channel_id=1, source_target_pairs={{0,4},{1,5},{2,6},{3,7},{4,0},{5,1},{6,2},{7,3},{8,12},{9,13},{10,... | collective-permute-start | bytes 1179656 | tf_op jit(solution)/shard_map/ppermute | solution.py:191
  169.1 9.8 %collective-permute-start.2 = (bf16[768,256]{1,0:T(8,128)(2,1)S(1)}, bf16[768,256]{1,0:T(8,128)(2,1)}, u32[]{:S(2)}, u32[]{:S(2)}) collective-permute-start(bf16[768,256]{1,0:T(8,128)(2,1)S(1)} %bitcast.17), channel_id=1, source_target_pairs={{0,6},{1,7},{2,0},{3,1},{4,2},{5,3},{6,4},{7,5},{8,14},{9,15},{10,... | collective-permute-start | bytes 1179656 | tf_op jit(solution)/shard_map/ppermute | solution.py:191
  173.1 32.0 %all-to-all-start.1 = ((f16[32,2,1152]{2,1,0:T(2,128)(2,1)}), f16[32,2,1152]{2,1,0:T(2,128)(2,1)S(1)}, u32[]{:S(2)}, u32[]{:S(2)}) async-start(f16[32,2,1152]{2,1,0:T(2,128)(2,1)} %broadcast_in_dim.3), calls=%async_computation.1 | async-start | bytes 294912 | tf_op jit(solution)/shard_map/all_to_all | solution.py:186
  177.9 6.7 %copy-start.2 = (bf16[4,256]{1,0:T(4,128)(2,1)S(1)}, bf16[4,256]{1,0:T(4,128)(2,1)}, u32[]{:S(2)}) copy-start(bf16[4,256]{1,0:T(4,128)(2,1)} %kn_ref.1) | copy-start | bytes 6148
  177.9 6.7 %copy-start.3 = (bf16[4,256]{1,0:T(4,128)(2,1)S(1)}, bf16[4,256]{1,0:T(4,128)(2,1)}, u32[]{:S(2)}) copy-start(bf16[4,256]{1,0:T(4,128)(2,1)} %vn_ref.1) | copy-start | bytes 6148
  177.9 6.7 %copy-start.4 = (f32[2]{0:T(128)S(1)}, f32[2]{0:T(128)}, u32[]{:S(2)}) copy-start(f32[2]{0:T(128)} %lam_ref.1) | copy-start | bytes 28
  177.9 6.7 %copy-start.5 = (f32[128]{0:T(128)S(1)}, f32[128]{0:T(128)}, u32[]{:S(2)}) copy-start(f32[128]{0:T(128)} %param.15) | copy-start | bytes 1540
  182.6 26.0 %collective-permute-start.4 = (f32[768,512]{1,0:T(8,128)}, f32[768,512]{1,0:T(8,128)}, u32[]{:S(2)}, u32[]{:S(2)}) collective-permute-start(f32[768,512]{1,0:T(8,128)} %shard_map.105), channel_id=1, source_target_pairs={{0,1},{1,0},{2,3},{3,2},{4,5},{5,4},{6,7},{7,6},{8,9},{9,8},{10,11... | collective-permute-start | bytes 4718600 | tf_op jit(solution)/shard_map/ppermute | solution.py:191
where the time goes:
time: 212 us; the launch traced here: 211 us
  blocking collectives  107 us (50%)
  waiting for transfers between devices  57 us (27%)
  starting transfers between devices  26.4 us (12%)
  Pallas kernels  13.2 us (6%)
  local copies, waits for them, and re-layouts  5 us (2%)
    all_gather x1, blocking collectives, inner(): w = lax.all_gather(w, 'sp', axis=0, tiled=True)  107 us
    all_to_all x2, waiting for transfers between devices, spread(): return lax.all_to_all(x, axis, 0, 0, tiled=True)  56.1 us
    ppermute x5, starting transfers between devices, moved(): return lax.ppermute(x, axis, [(i, step(i) % n) for i in range(n)])  15.6 us
    pallas_call x6, Pallas kernels, call(): pl.pallas_call(kernel, out_shape=[jax.ShapeDtypeStruct(s, d) for s, d in...  13.2 us
    all_to_all x2, starting transfers between devices, spread(): return lax.all_to_all(x, axis, 0, 0, tiled=True)  10.7 us
  transfers between devices with their start and end apart: 7, of which 3 were waited for; matrix products, arithmetic and copies ran while one was open for 1% of the time, Pallas kernels for 4%

commit v1 on v0

--- a/solution.py
+++ b/solution.py
@@ -30,7 +30,11 @@
     return jnp.where(lane // HALF == slot, out, 0.0)
 
 
-def local_kernel(heads, x_ref, w_ref, q_ref, pay_ref):
+def local_kernel(heads, x_ref, blocks_ref, w_ref, q_ref, pay_ref, mine_ref, sem):
+    depth = mine_ref.shape[2]
+    lanes = pl.ds(pl.multiple_of(lax.axis_index("tp") * depth, depth), depth)
+    cut = pltpu.make_async_copy(blocks_ref.at[:, :, lanes], mine_ref, sem)
+    cut.start()
     count, piece, width = x_ref.shape
     rows = 2 * count * heads
     cols = heads * 2 * HALF
@@ -58,6 +62,7 @@
     pay_ref[rows:, :] = jnp.zeros((pay_ref.shape[0] - rows, VDIM), F32)
     pieces = [p.astype(F32) * 256.0**n for x in (top / 64, total) for n, p in enumerate(three(x))]
     pay_ref[rows : rows + 1, :] = as_line([*pieces, power])
+    cut.wait()
 
 
 def three(x):
@@ -203,10 +208,8 @@
     t = lax.axis_index("tp")
 
     depth = width // slices
-    mine = lax.dynamic_slice_in_dim(prompt, t * depth, depth, 2).reshape(peers, sub, depth)
     w = jnp.concatenate([w_key, w_value], axis=1)
     w = (w.astype(F32) * W_SHIFT).astype(jnp.float16)
-    mine, w = lax.optimization_barrier((mine, w))
     w = lax.all_gather(w, "sp", axis=0, tiled=True)
     w = (w.astype(F32) * (1 / W_SHIFT)).astype(BF16)
 
@@ -217,8 +220,13 @@
         "s",
     )
     each = half + 1
-    (pay,) = call(functools.partial(local_kernel, heads), [((2 * each, VDIM), F32)], (prompt, w, query_new))
-    pay, mine = lax.optimization_barrier((pay, mine))
+    pay, mine = call(
+        functools.partial(local_kernel, heads),
+        [((2 * each, VDIM), F32), ((peers, sub, depth), BF16)],
+        (prompt, prompt.reshape(peers, sub, width), w, query_new),
+        "va",
+        [pltpu.SemaphoreType.DMA],
+    )
     mine = spread(mine, "sp").reshape(peers * sub, depth)
     parts = jnp.broadcast_to(pay.reshape(2, each * VDIM).astype(jnp.float16), (peers, 2, each * VDIM))
     parts = spread(parts, "sp")

time: 212 us -> 211 us (level)
  no operation moved by 1% of the time
where the time goes in v1:
time: 211 us; the launch traced here: 210 us
  blocking collectives  107 us (51%)
  waiting for transfers between devices  57 us (27%)
  starting transfers between devices  26.3 us (12%)
  Pallas kernels  14 us (7%)
  local copies, waits for them, and re-layouts  3.22 us (2%)
    all_gather x1, blocking collectives, inner(): w = lax.all_gather(w, 'sp', axis=0, tiled=True)  107 us
    all_to_all x2, waiting for transfers between devices, spread(): return lax.all_to_all(x, axis, 0, 0, tiled=True)  56 us
    ppermute x5, starting transfers between devices, moved(): return lax.ppermute(x, axis, [(i, step(i) % n) for i in range(n)])  15.6 us
    pallas_call x6, Pallas kernels, call(): pl.pallas_call(kernel, out_shape=[jax.ShapeDtypeStruct(s, d) for s, d in...  14 us
    all_to_all x2, starting transfers between devices, spread(): return lax.all_to_all(x, axis, 0, 0, tiled=True)  10.7 us
  transfers between devices with their start and end apart: 7, of which 3 were waited for; matrix products, arithmetic and copies ran while one was open for 1% of the time, Pallas kernels for 4%

profile of v1, /device:TPU:40, one launch (start us, length us, event | category | flops | bytes accessed | tf_op | source)
XLA Modules:
  0.0 210.2 jit_solution(12157820281599506470)
XLA Ops:
  0.6 0.8 multiply_convert_fusion.1
  1.4 107.4 %all-gather.1 = f16[2048,512]{1,0:T(8,128)(2,1)S(1)} all-gather(f16[64,512]{1,0:T(8,128)(2,1)S(1)} %multiply_convert_fusion.1), channel_id=1, replica_groups=mesh['grp'=2,'sp'=32,'tp'=8] {'sp'}, dimensions={0}, use_global_device_ids=true | all-gather | bytes 2162688 | tf_op jit(solution)/shard_map/all_gather | solution.py:213
  108.9 0.5 multiply_convert_fusion.w_ref
  109.4 1.4 copy-done
  110.7 0.0 copy-done.1
  110.7 3.5 %shard_map.103 = (f32[18,128]{1,0:T(8,128)S(1)}, bf16[32,24,256]{2,1,0:T(8,128)(2,1)}) custom-call(bf16[4,192,2048]{2,1,0:T(8,128)(2,1)S(1)} %copy-done, bf16[32,24,2048]{2,1,0:T(8,128)(2,1)S(1)} %bitcast.15, bf16[2048,512]{1,0:T(8,128)(2,1)S(1)} %multiply_convert_fusion.w_ref, bf16[4,256]{1,0:T(4,128)(2,1)S(1)} %copy-done.1), custom_call_target="tpu_custom_call" | custom-call | tf_op jit(solution)/shard_map/pallas_call | solution.py:180
  114.2 5.9 %all-to-all-start = ((bf16[32,24,256]{2,1,0:T(8,128)(2,1)}), bf16[32,24,256]{2,1,0:T(8,128)(2,1)S(1)}, u32[]{:S(2)}, u32[]{:S(2)}) async-start(bf16[32,24,256]{2,1,0:T(8,128)(2,1)} %get-tuple-element.7), calls=%async_computation | async-start | bytes 786432 | tf_op jit(solution)/shard_map/all_to_all | solution.py:191
  120.2 1.0 dynamic-slice_bitcast_fusion
  121.3 1.9 collective-permute-start.3
  123.2 36.4 %all-to-all-done = bf16[32,24,256]{2,1,0:T(8,128)(2,1)S(1)} async-done(((bf16[32,24,256]{2,1,0:T(8,128)(2,1)}), bf16[32,24,256]{2,1,0:T(8,128)(2,1)S(1)}, u32[]{:S(2)}, u32[]{:S(2)}) %all-to-all-start) | async-done | bytes 393248 | tf_op jit(solution)/shard_map/all_to_all | solution.py:191
  159.6 3.6 %collective-permute-start = (bf16[768,256]{1,0:T(8,128)(2,1)S(1)}, bf16[768,256]{1,0:T(8,128)(2,1)S(1)}, u32[]{:S(2)}, u32[]{:S(2)}) collective-permute-start(bf16[768,256]{1,0:T(8,128)(2,1)S(1)} %bitcast.16), channel_id=1, source_target_pairs={{0,2},{1,3},{2,4},{3,5},{4,6},{5,7},{6,0},{7,1},{8,10},{9,11},{10,... | collective-permute-start | bytes 1179656 | tf_op jit(solution)/shard_map/ppermute | solution.py:196
  163.2 4.9 %collective-permute-start.1 = (bf16[768,256]{1,0:T(8,128)(2,1)S(1)}, bf16[768,256]{1,0:T(8,128)(2,1)S(1)}, u32[]{:S(2)}, u32[]{:S(2)}) collective-permute-start(bf16[768,256]{1,0:T(8,128)(2,1)S(1)} %bitcast.17), channel_id=1, source_target_pairs={{0,4},{1,5},{2,6},{3,7},{4,0},{5,1},{6,2},{7,3},{8,12},{9,13},{10,... | collective-permute-start | bytes 1179656 | tf_op jit(solution)/shard_map/ppermute | solution.py:196
  168.1 3.2 %collective-permute-start.2 = (bf16[768,256]{1,0:T(8,128)(2,1)S(1)}, bf16[768,256]{1,0:T(8,128)(2,1)}, u32[]{:S(2)}, u32[]{:S(2)}) collective-permute-start(bf16[768,256]{1,0:T(8,128)(2,1)S(1)} %bitcast.18), channel_id=1, source_target_pairs={{0,6},{1,7},{2,0},{3,1},{4,2},{5,3},{6,4},{7,5},{8,14},{9,15},{10,... | collective-permute-start | bytes 1179656 | tf_op jit(solution)/shard_map/ppermute | solution.py:196
  171.4 0.7 broadcast_in_dim.3
  172.1 4.8 %all-to-all-start.1 = ((f16[32,2,1152]{2,1,0:T(2,128)(2,1)}), f16[32,2,1152]{2,1,0:T(2,128)(2,1)S(1)}, u32[]{:S(2)}, u32[]{:S(2)}) async-start(f16[32,2,1152]{2,1,0:T(2,128)(2,1)} %broadcast_in_dim.3), calls=%async_computation.1 | async-start | bytes 294912 | tf_op jit(solution)/shard_map/all_to_all | solution.py:191
  176.9 0.0 copy-start.2
  176.9 0.0 copy-start.3
  176.9 0.0 copy-start.4
  176.9 0.0 copy-start.5
  177.0 0.0 collective-permute-done.3.refs_4_
  177.0 0.0 collective-permute-done.refs_1_
  177.0 0.0 collective-permute-done.1.refs_2_
  177.0 0.9 collective-permute-done.2.refs_3_
  177.9 3.8 %shard_map.105 = f32[768,512]{1,0:T(8,128)} custom-call(bf16[768,256]{1,0:T(8,128)(2,1)S(1)} %bitcast.19, bf16[768,256]{1,0:T(8,128)(2,1)S(1)} %collective-permute-done.refs_1_, bf16[768,256]{1,0:T(8,128)(2,1)S(1)} %collective-permute-done.1.refs_2_, bf16[768,256]{1,0:T(8,128)(2,1)} %collective-permute-done.2.refs_3_, ...), custom_call_target="tpu_custom_call" | custom-call | tf_op jit(solution)/shard_map/pallas_call | solution.py:180
  181.7 2.0 collective-permute-start.4
  183.7 0.0 copy-done.2
  183.7 0.8 shard_map.107.new_ref
  184.5 19.7 %all-to-all-done.1 = f16[32,2,1152]{2,1,0:T(2,128)(2,1)S(1)} async-done(((f16[32,2,1152]{2,1,0:T(2,128)(2,1)}), f16[32,2,1152]{2,1,0:T(2,128)(2,1)S(1)}, u32[]{:S(2)}, u32[]{:S(2)}) %all-to-all-start.1) | async-done | bytes 147488 | tf_op jit(solution)/shard_map/all_to_all | solution.py:191
  204.2 1.0 shard_map.108
  205.1 2.5 %shard_map.104.ours_ref = f32[768,512]{1,0:T(8,128)S(1)} custom-call(bf16[768,256]{1,0:T(8,128)(2,1)S(1)} %bitcast.20, bf16[768,256]{1,0:T(8,128)(2,1)S(1)} %collective-permute-done.refs_1_, bf16[768,256]{1,0:T(8,128)(2,1)S(1)} %collective-permute-done.1.refs_2_, bf16[768,256]{1,0:T(8,128)(2,1)} %collective-permute-done.2.refs_3_, ...), custom_call_target="tpu_custom_call" | custom-call | tf_op jit(solution)/shard_map/pallas_call | solution.py:180
  207.7 0.0 collective-permute-done.4.swapped_ref
  207.7 2.5 %shard_map.106 = (bf16[768,256]{1,0:T(8,128)(2,1)}, bf16[768,256]{1,0:T(8,128)(2,1)}) custom-call(f32[768,512]{1,0:T(8,128)S(1)} %shard_map.104.ours_ref, f32[768,512]{1,0:T(8,128)} %collective-permute-done.4.swapped_ref), custom_call_target="tpu_custom_call" | custom-call | tf_op jit(solution)/shard_map/pallas_call | solution.py:180
  (8 shorter events, 0.1 us)
Async XLA Ops:
  108.9 1.9 copy-start
  108.9 1.9 copy-start.1
  114.2 45.3 %all-to-all-start = ((bf16[32,24,256]{2,1,0:T(8,128)(2,1)}), bf16[32,24,256]{2,1,0:T(8,128)(2,1)S(1)}, u32[]{:S(2)}, u32[]{:S(2)}) async-start(bf16[32,24,256]{2,1,0:T(8,128)(2,1)} %get-tuple-element.7), calls=%async_computation | async-start | bytes 786432 | tf_op jit(solution)/shard_map/all_to_all | solution.py:191
  121.3 55.7 %collective-permute-start.3 = (bf16[4,256,512]{2,1,0:T(8,128)(2,1)}, bf16[4,256,512]{2,1,0:T(8,128)(2,1)}, u32[]{:S(2)}, u32[]{:S(2)}) collective-permute-start(bf16[4,256,512]{2,1,0:T(8,128)(2,1)} %dynamic-slice_bitcast_fusion), channel_id=1, source_target_pairs={{0,1},{1,0},{2,3},{3,2},{4,5},{5,4},{6,7},{7,6},{8,9},{9,8},{10,11... | collective-permute-start | bytes 3145736 | tf_op jit(solution)/shard_map/ppermute | solution.py:196
  159.6 17.4 %collective-permute-start = (bf16[768,256]{1,0:T(8,128)(2,1)S(1)}, bf16[768,256]{1,0:T(8,128)(2,1)S(1)}, u32[]{:S(2)}, u32[]{:S(2)}) collective-permute-start(bf16[768,256]{1,0:T(8,128)(2,1)S(1)} %bitcast.16), channel_id=1, source_target_pairs={{0,2},{1,3},{2,4},{3,5},{4,6},{5,7},{6,0},{7,1},{8,10},{9,11},{10,... | collective-permute-start | bytes 1179656 | tf_op jit(solution)/shard_map/ppermute | solution.py:196
  163.2 13.8 %collective-permute-start.1 = (bf16[768,256]{1,0:T(8,128)(2,1)S(1)}, bf16[768,256]{1,0:T(8,128)(2,1)S(1)}, u32[]{:S(2)}, u32[]{:S(2)}) collective-permute-start(bf16[768,256]{1,0:T(8,128)(2,1)S(1)} %bitcast.17), channel_id=1, source_target_pairs={{0,4},{1,5},{2,6},{3,7},{4,0},{5,1},{6,2},{7,3},{8,12},{9,13},{10,... | collective-permute-start | bytes 1179656 | tf_op jit(solution)/shard_map/ppermute | solution.py:196
  168.1 9.8 %collective-permute-start.2 = (bf16[768,256]{1,0:T(8,128)(2,1)S(1)}, bf16[768,256]{1,0:T(8,128)(2,1)}, u32[]{:S(2)}, u32[]{:S(2)}) collective-permute-start(bf16[768,256]{1,0:T(8,128)(2,1)S(1)} %bitcast.18), channel_id=1, source_target_pairs={{0,6},{1,7},{2,0},{3,1},{4,2},{5,3},{6,4},{7,5},{8,14},{9,15},{10,... | collective-permute-start | bytes 1179656 | tf_op jit(solution)/shard_map/ppermute | solution.py:196
  172.1 32.0 %all-to-all-start.1 = ((f16[32,2,1152]{2,1,0:T(2,128)(2,1)}), f16[32,2,1152]{2,1,0:T(2,128)(2,1)S(1)}, u32[]{:S(2)}, u32[]{:S(2)}) async-start(f16[32,2,1152]{2,1,0:T(2,128)(2,1)} %broadcast_in_dim.3), calls=%async_computation.1 | async-start | bytes 294912 | tf_op jit(solution)/shard_map/all_to_all | solution.py:191
  176.9 6.8 %copy-start.2 = (bf16[4,256]{1,0:T(4,128)(2,1)S(1)}, bf16[4,256]{1,0:T(4,128)(2,1)}, u32[]{:S(2)}) copy-start(bf16[4,256]{1,0:T(4,128)(2,1)} %kn_ref.1) | copy-start | bytes 6148
  176.9 6.8 %copy-start.3 = (bf16[4,256]{1,0:T(4,128)(2,1)S(1)}, bf16[4,256]{1,0:T(4,128)(2,1)}, u32[]{:S(2)}) copy-start(bf16[4,256]{1,0:T(4,128)(2,1)} %vn_ref.1) | copy-start | bytes 6148
  176.9 6.8 %copy-start.4 = (f32[2]{0:T(128)S(1)}, f32[2]{0:T(128)}, u32[]{:S(2)}) copy-start(f32[2]{0:T(128)} %lam_ref.1) | copy-start | bytes 28
  176.9 6.8 %copy-start.5 = (f32[128]{0:T(128)S(1)}, f32[128]{0:T(128)}, u32[]{:S(2)}) copy-start(f32[128]{0:T(128)} %param.15) | copy-start | bytes 1540
  181.7 26.0 %collective-permute-start.4 = (f32[768,512]{1,0:T(8,128)}, f32[768,512]{1,0:T(8,128)}, u32[]{:S(2)}, u32[]{:S(2)}) collective-permute-start(f32[768,512]{1,0:T(8,128)} %shard_map.105), channel_id=1, source_target_pairs={{0,1},{1,0},{2,3},{3,2},{4,5},{5,4},{6,7},{7,6},{8,9},{9,8},{10,11... | collective-permute-start | bytes 4718600 | tf_op jit(solution)/shard_map/ppermute | solution.py:196

commit v2 on v1

--- a/solution.py
+++ b/solution.py
@@ -30,17 +30,24 @@
     return jnp.where(lane // HALF == slot, out, 0.0)
 
 
-def local_kernel(heads, x_ref, blocks_ref, w_ref, q_ref, pay_ref, mine_ref, sem):
+def project_kernel(x_ref, blocks_ref, w_ref, keys_ref, values_ref, mine_ref, sem):
+    count, piece, width = x_ref.shape
+    cols = keys_ref.shape[1]
     depth = mine_ref.shape[2]
     lanes = pl.ds(pl.multiple_of(lax.axis_index("tp") * depth, depth), depth)
     cut = pltpu.make_async_copy(blocks_ref.at[:, :, lanes], mine_ref, sem)
     cut.start()
-    count, piece, width = x_ref.shape
+    x = x_ref[...].reshape(count * piece, width)
+    keys_ref[...] = jnp.dot(x, w_ref[:, :cols], preferred_element_type=F32).astype(BF16)
+    values_ref[...] = jnp.dot(x, w_ref[:, cols:], preferred_element_type=F32).astype(BF16)
+    cut.wait()
+
+
+def local_kernel(heads, keys_ref, values_ref, q_ref, pay_ref):
+    count = q_ref.shape[0]
+    piece = keys_ref.shape[0] // count
     rows = 2 * count * heads
-    cols = heads * 2 * HALF
-    x = x_ref[...].reshape(count * piece, width)
-    keys = jnp.dot(x, w_ref[:, :cols], preferred_element_type=F32).astype(BF16)
-    values = jnp.dot(x, w_ref[:, cols:], preferred_element_type=F32).astype(BF16)
+    keys, values = keys_ref[...], values_ref[...]
     picked = select_rows(rows, q_ref[...], count, heads, 2)
     scores = row_dot(picked.astype(BF16), keys) * HALF**-0.5
     r = lax.broadcasted_iota(jnp.int32, scores.shape, 0)
@@ -62,7 +69,6 @@
     pay_ref[rows:, :] = jnp.zeros((pay_ref.shape[0] - rows, VDIM), F32)
     pieces = [p.astype(F32) * 256.0**n for x in (top / 64, total) for n, p in enumerate(three(x))]
     pay_ref[rows : rows + 1, :] = as_line([*pieces, power])
-    cut.wait()
 
 
 def three(x):
@@ -220,14 +226,15 @@
         "s",
     )
     each = half + 1
-    pay, mine = call(
-        functools.partial(local_kernel, heads),
-        [((2 * each, VDIM), F32), ((peers, sub, depth), BF16)],
-        (prompt, prompt.reshape(peers, sub, width), w, query_new),
+    keys, values, mine = call(
+        project_kernel,
+        [((count * piece, cols), BF16)] * 2 + [((peers, sub, depth), BF16)],
+        (prompt, prompt.reshape(peers, sub, width), w),
         "va",
         [pltpu.SemaphoreType.DMA],
     )
     mine = spread(mine, "sp").reshape(peers * sub, depth)
+    (pay,) = call(functools.partial(local_kernel, heads), [((2 * each, VDIM), F32)], (keys, values, query_new))
     parts = jnp.broadcast_to(pay.reshape(2, each * VDIM).astype(jnp.float16), (peers, 2, each * VDIM))
     parts = spread(parts, "sp")
     parts = parts.astype(F32).transpose(1, 0, 2)

time: 211 us -> 214 us (1.014)
  the two profiles are of different devices: /device:TPU:40 before, /device:TPU:34 now
where the time goes in v2:
time: 214 us; the launch traced here: 213 us
  blocking collectives  107 us (50%)
  waiting for transfers between devices  57.1 us (27%)
  starting transfers between devices  25.6 us (12%)
  Pallas kernels  13.7 us (6%)
  local copies, waits for them, and re-layouts  6.77 us (3%)
    all_gather x1, blocking collectives, inner(): w = lax.all_gather(w, 'sp', axis=0, tiled=True)  107 us
    all_to_all x2, waiting for transfers between devices, spread(): return lax.all_to_all(x, axis, 0, 0, tiled=True)  57.1 us
    ppermute x5, starting transfers between devices, moved(): return lax.ppermute(x, axis, [(i, step(i) % n) for i in range(n)])  14.7 us
    pallas_call x7, Pallas kernels, call(): pl.pallas_call(kernel, out_shape=[jax.ShapeDtypeStruct(s, d) for s, d in...  13.7 us
    all_to_all x2, starting transfers between devices, spread(): return lax.all_to_all(x, axis, 0, 0, tiled=True)  10.8 us
    unnamed x20, local copies, waits for them, and re-layouts  4.91 us
  transfers between devices with their start and end apart: 7, of which 2 were waited for; matrix products, arithmetic and copies ran while one was open for 1% of the time, Pallas kernels for 4%

profile of v2, /device:TPU:34, one launch (start us, length us, event | category | flops | bytes accessed | tf_op | source)
XLA Modules:
  0.0 212.8 jit_solution(8896588711787378777)
XLA Ops:
  0.6 0.8 multiply_convert_fusion.1
  1.4 107.4 %all-gather.1 = f16[2048,512]{1,0:T(8,128)(2,1)S(1)} all-gather(f16[64,512]{1,0:T(8,128)(2,1)S(1)} %multiply_convert_fusion.1), channel_id=1, replica_groups=mesh['grp'=2,'sp'=32,'tp'=8] {'sp'}, dimensions={0}, use_global_device_ids=true | all-gather | bytes 2162688 | tf_op jit(solution)/shard_map/all_gather | solution.py:219
  108.9 0.5 multiply_convert_fusion.w_ref
  109.4 1.4 copy-done
  110.7 2.6 %shard_map.103 = (bf16[768,256]{1,0:T(8,128)(2,1)S(1)}, bf16[768,256]{1,0:T(8,128)(2,1)S(1)}, bf16[32,24,256]{2,1,0:T(8,128)(2,1)}) custom-call(bf16[4,192,2048]{2,1,0:T(8,128)(2,1)S(1)} %copy-done, bf16[32,24,2048]{2,1,0:T(8,128)(2,1)S(1)} %bitcast.15, bf16[2048,512]{1,0:T(8,128)(2,1)S(1)} %multiply_convert_fusion.w_ref), custom_call_target="tpu_custom_call" | custom-call | tf_op jit(solution)/shard_map/pallas_call | solution.py:186
  113.4 0.0 copy-start.1
  113.4 0.7 copy-done.1
  114.1 0.8 copy-done.3
  114.9 6.1 %all-to-all-start = ((bf16[32,24,256]{2,1,0:T(8,128)(2,1)}), bf16[32,24,256]{2,1,0:T(8,128)(2,1)S(1)}, u32[]{:S(2)}, u32[]{:S(2)}) async-start(bf16[32,24,256]{2,1,0:T(8,128)(2,1)} %get-tuple-element.8), calls=%async_computation | async-start | bytes 786432 | tf_op jit(solution)/shard_map/all_to_all | solution.py:197
  121.0 1.1 dynamic-slice_bitcast_fusion
  122.0 1.9 collective-permute-start.3
  124.0 36.4 %all-to-all-done = bf16[32,24,256]{2,1,0:T(8,128)(2,1)S(1)} async-done(((bf16[32,24,256]{2,1,0:T(8,128)(2,1)}), bf16[32,24,256]{2,1,0:T(8,128)(2,1)S(1)}, u32[]{:S(2)}, u32[]{:S(2)}) %all-to-all-start) | async-done | bytes 393248 | tf_op jit(solution)/shard_map/all_to_all | solution.py:197
  160.3 2.3 %collective-permute-start.2 = (bf16[768,256]{1,0:T(8,128)(2,1)S(1)}, bf16[768,256]{1,0:T(8,128)(2,1)S(1)}, u32[]{:S(2)}, u32[]{:S(2)}) collective-permute-start(bf16[768,256]{1,0:T(8,128)(2,1)S(1)} %bitcast.16), channel_id=1, source_target_pairs={{0,6},{1,7},{2,0},{3,1},{4,2},{5,3},{6,4},{7,5},{8,14},{9,15},{10,... | collective-permute-start | bytes 1179656 | tf_op jit(solution)/shard_map/ppermute | solution.py:202
  162.7 4.6 %collective-permute-start.1 = (bf16[768,256]{1,0:T(8,128)(2,1)S(1)}, bf16[768,256]{1,0:T(8,128)(2,1)S(1)}, u32[]{:S(2)}, u32[]{:S(2)}) collective-permute-start(bf16[768,256]{1,0:T(8,128)(2,1)S(1)} %bitcast.17), channel_id=1, source_target_pairs={{0,4},{1,5},{2,6},{3,7},{4,0},{5,1},{6,2},{7,3},{8,12},{9,13},{10,... | collective-permute-start | bytes 1179656 | tf_op jit(solution)/shard_map/ppermute | solution.py:202
  167.3 3.9 %collective-permute-start = (bf16[768,256]{1,0:T(8,128)(2,1)S(1)}, bf16[768,256]{1,0:T(8,128)(2,1)}, u32[]{:S(2)}, u32[]{:S(2)}) collective-permute-start(bf16[768,256]{1,0:T(8,128)(2,1)S(1)} %bitcast.18), channel_id=1, source_target_pairs={{0,2},{1,3},{2,4},{3,5},{4,6},{5,7},{6,0},{7,1},{8,10},{9,11},{10,... | collective-permute-start | bytes 1179656 | tf_op jit(solution)/shard_map/ppermute | solution.py:202
  171.2 0.0 copy-start.2
  171.2 1.0 copy-done.2
  172.2 1.0 copy-done.4
  173.2 0.9 shard_map.107
  174.2 0.7 broadcast_in_dim.3
  175.0 4.8 %all-to-all-start.1 = ((f16[32,2,1152]{2,1,0:T(2,128)(2,1)}), f16[32,2,1152]{2,1,0:T(2,128)(2,1)S(1)}, u32[]{:S(2)}, u32[]{:S(2)}) async-start(f16[32,2,1152]{2,1,0:T(2,128)(2,1)} %broadcast_in_dim.3), calls=%async_computation.1 | async-start | bytes 294912 | tf_op jit(solution)/shard_map/all_to_all | solution.py:197
  179.7 0.0 copy-start.6
  179.7 0.0 copy-start.7
  179.8 0.0 copy-start.8
  179.8 0.0 copy-start.9
  179.8 3.6 %shard_map.105 = f32[768,512]{1,0:T(8,128)} custom-call(bf16[768,256]{1,0:T(8,128)(2,1)S(1)} %bitcast.19, bf16[768,256]{1,0:T(8,128)(2,1)} %collective-permute-done.refs_1_, bf16[768,256]{1,0:T(8,128)(2,1)S(1)} %collective-permute-done.1.refs_2_, bf16[768,256]{1,0:T(8,128)(2,1)S(1)} %collective-permute-done.2.refs_3_, ...), custom_call_target="tpu_custom_call" | custom-call | tf_op jit(solution)/shard_map/pallas_call | solution.py:186
  183.5 2.0 collective-permute-start.4
  185.5 0.8 shard_map.108.new_ref
  186.2 20.8 %all-to-all-done.1 = f16[32,2,1152]{2,1,0:T(2,128)(2,1)S(1)} async-done(((f16[32,2,1152]{2,1,0:T(2,128)(2,1)}), f16[32,2,1152]{2,1,0:T(2,128)(2,1)S(1)}, u32[]{:S(2)}, u32[]{:S(2)}) %all-to-all-start.1) | async-done | bytes 147488 | tf_op jit(solution)/shard_map/all_to_all | solution.py:197
  207.0 1.0 shard_map.109
  208.0 2.4 %shard_map.104.ours_ref = f32[768,512]{1,0:T(8,128)S(1)} custom-call(bf16[768,256]{1,0:T(8,128)(2,1)S(1)} %bitcast.20, bf16[768,256]{1,0:T(8,128)(2,1)} %collective-permute-done.refs_1_, bf16[768,256]{1,0:T(8,128)(2,1)S(1)} %collective-permute-done.1.refs_2_, bf16[768,256]{1,0:T(8,128)(2,1)S(1)} %collective-permute-done.2.refs_3_, ...), custom_call_target="tpu_custom_call" | custom-call | tf_op jit(solution)/shard_map/pallas_call | solution.py:186
  210.4 2.5 %shard_map.106 = (bf16[768,256]{1,0:T(8,128)(2,1)}, bf16[768,256]{1,0:T(8,128)(2,1)}) custom-call(f32[768,512]{1,0:T(8,128)S(1)} %shard_map.104.ours_ref, f32[768,512]{1,0:T(8,128)} %collective-permute-done.4.swapped_ref), custom_call_target="tpu_custom_call" | custom-call | tf_op jit(solution)/shard_map/pallas_call | solution.py:186
  (17 shorter events, 0.1 us)
Async XLA Ops:
  108.9 1.9 copy-start
  113.4 0.7 copy-start.1
  114.1 0.8 copy-start.3
  114.9 56.3 %copy-start.5 = (bf16[4,256]{1,0:T(4,128)(2,1)S(1)}, bf16[4,256]{1,0:T(4,128)(2,1)}, u32[]{:S(2)}) copy-start(bf16[4,256]{1,0:T(4,128)(2,1)} %q_ref.3) | copy-start | bytes 6148
  114.9 45.5 %all-to-all-start = ((bf16[32,24,256]{2,1,0:T(8,128)(2,1)}), bf16[32,24,256]{2,1,0:T(8,128)(2,1)S(1)}, u32[]{:S(2)}, u32[]{:S(2)}) async-start(bf16[32,24,256]{2,1,0:T(8,128)(2,1)} %get-tuple-element.8), calls=%async_computation | async-start | bytes 786432 | tf_op jit(solution)/shard_map/all_to_all | solution.py:197
  122.0 57.7 %collective-permute-start.3 = (bf16[4,256,512]{2,1,0:T(8,128)(2,1)}, bf16[4,256,512]{2,1,0:T(8,128)(2,1)}, u32[]{:S(2)}, u32[]{:S(2)}) collective-permute-start(bf16[4,256,512]{2,1,0:T(8,128)(2,1)} %dynamic-slice_bitcast_fusion), channel_id=1, source_target_pairs={{0,1},{1,0},{2,3},{3,2},{4,5},{5,4},{6,7},{7,6},{8,9},{9,8},{10,11... | collective-permute-start | bytes 3145736 | tf_op jit(solution)/shard_map/ppermute | solution.py:202
  160.3 19.4 %collective-permute-start.2 = (bf16[768,256]{1,0:T(8,128)(2,1)S(1)}, bf16[768,256]{1,0:T(8,128)(2,1)S(1)}, u32[]{:S(2)}, u32[]{:S(2)}) collective-permute-start(bf16[768,256]{1,0:T(8,128)(2,1)S(1)} %bitcast.16), channel_id=1, source_target_pairs={{0,6},{1,7},{2,0},{3,1},{4,2},{5,3},{6,4},{7,5},{8,14},{9,15},{10,... | collective-permute-start | bytes 1179656 | tf_op jit(solution)/shard_map/ppermute | solution.py:202
  162.7 17.1 %collective-permute-start.1 = (bf16[768,256]{1,0:T(8,128)(2,1)S(1)}, bf16[768,256]{1,0:T(8,128)(2,1)S(1)}, u32[]{:S(2)}, u32[]{:S(2)}) collective-permute-start(bf16[768,256]{1,0:T(8,128)(2,1)S(1)} %bitcast.17), channel_id=1, source_target_pairs={{0,4},{1,5},{2,6},{3,7},{4,0},{5,1},{6,2},{7,3},{8,12},{9,13},{10,... | collective-permute-start | bytes 1179656 | tf_op jit(solution)/shard_map/ppermute | solution.py:202
  167.3 12.5 %collective-permute-start = (bf16[768,256]{1,0:T(8,128)(2,1)S(1)}, bf16[768,256]{1,0:T(8,128)(2,1)}, u32[]{:S(2)}, u32[]{:S(2)}) collective-permute-start(bf16[768,256]{1,0:T(8,128)(2,1)S(1)} %bitcast.18), channel_id=1, source_target_pairs={{0,2},{1,3},{2,4},{3,5},{4,6},{5,7},{6,0},{7,1},{8,10},{9,11},{10,... | collective-permute-start | bytes 1179656 | tf_op jit(solution)/shard_map/ppermute | solution.py:202
  171.2 1.0 copy-start.2
  172.2 1.0 copy-start.4
  175.0 32.0 %all-to-all-start.1 = ((f16[32,2,1152]{2,1,0:T(2,128)(2,1)}), f16[32,2,1152]{2,1,0:T(2,128)(2,1)S(1)}, u32[]{:S(2)}, u32[]{:S(2)}) async-start(f16[32,2,1152]{2,1,0:T(2,128)(2,1)} %broadcast_in_dim.3), calls=%async_computation.1 | async-start | bytes 294912 | tf_op jit(solution)/shard_map/all_to_all | solution.py:197
  179.7 5.7 %copy-start.6 = (bf16[4,256]{1,0:T(4,128)(2,1)S(1)}, bf16[4,256]{1,0:T(4,128)(2,1)}, u32[]{:S(2)}) copy-start(bf16[4,256]{1,0:T(4,128)(2,1)} %kn_ref.1) | copy-start | bytes 6148
  179.7 5.7 %copy-start.7 = (bf16[4,256]{1,0:T(4,128)(2,1)S(1)}, bf16[4,256]{1,0:T(4,128)(2,1)}, u32[]{:S(2)}) copy-start(bf16[4,256]{1,0:T(4,128)(2,1)} %vn_ref.1) | copy-start | bytes 6148
  179.8 5.7 %copy-start.8 = (f32[2]{0:T(128)S(1)}, f32[2]{0:T(128)}, u32[]{:S(2)}) copy-start(f32[2]{0:T(128)} %lam_ref.1) | copy-start | bytes 28
  179.8 5.7 %copy-start.9 = (f32[128]{0:T(128)S(1)}, f32[128]{0:T(128)}, u32[]{:S(2)}) copy-start(f32[128]{0:T(128)} %param.15) | copy-start | bytes 1540
  183.5 26.9 %collective-permute-start.4 = (f32[768,512]{1,0:T(8,128)}, f32[768,512]{1,0:T(8,128)}, u32[]{:S(2)}, u32[]{:S(2)}) collective-permute-start(f32[768,512]{1,0:T(8,128)} %shard_map.105), channel_id=1, source_target_pairs={{0,1},{1,0},{2,3},{3,2},{4,5},{5,4},{6,7},{7,6},{8,9},{9,8},{10,11... | collective-permute-start | bytes 4718600 | tf_op jit(solution)/shard_map/ppermute | solution.py:202
